TPU v7x, 32 devices: a whole 2x2x4 slice. The times are simulated.
32 devices in a mesh: fs: 4 (over y, x), tp: 8 (over z, core).
Axes of the slice: x: 2, y: 2, z: 4, core: 2. Of those that a mesh axis runs over, the one named last changes fastest.
Arguments:
- saved_query_latent: bfloat16 [4096, 1536], P('fs', 'tp'), may hold values from -6 to 6
- saved_key_value_latent: bfloat16 [4096, 1024], P('fs', 'tp'), may hold values from -6 to 6
- query_cot: bfloat16 [4096, 6144], P('fs', 'tp'), may hold values from -0.09375 to 0.09375
- kv_cot: bfloat16 [4096, 8192], P('fs', 'tp'), may hold values from -0.09375 to 0.09375
- query_full_weight: float32 [1536, 6144], P('fs', 'tp'), may hold values from -0.6 to 0.6
- key_value_full_weight: float32 [1024, 8192], P('fs', 'tp'), may hold values from -0.6 to 0.6
- query_mom: float32 [1536, 6144], P('fs', 'tp'), may hold values from -50 to 50
- kv_mom: float32 [1024, 8192], P('fs', 'tp'), may hold values from -50 to 50
- query_left: bfloat16 [1536, 1536], P('fs'), may hold values from -1 to 1.5
- kv_left: bfloat16 [1024, 1024], P('fs'), may hold values from -1 to 1.5
- query_right: bfloat16 [32, 192, 192], P('tp'), may hold values from -1 to 1.5
- kv_right: bfloat16 [32, 256, 256], P('tp'), may hold values from -1 to 1.5
Outputs:
- query_mom_new: float32 [1536, 6144], P('fs', 'tp')
- kv_mom_new: float32 [1024, 8192], P('fs', 'tp')
- query_update: float32 [1536, 6144], P('fs', 'tp')
- kv_update: float32 [1024, 8192], P('fs', 'tp')
- query_weight: float32 [1536, 6144], P('fs', 'tp')
- kv_weight: float32 [1024, 8192], P('fs', 'tp')
- query_copy: bfloat16 [1536, 6144], P(None, 'tp')
- kv_copy: bfloat16 [1024, 8192], P(None, 'tp')
All inputs are finite; a program needn't handle non-finite values.
Results may differ from a plain program's by a relative error of at most 0.0055.
Values may be sent and summed in bfloat16 or wider, within the bound.
A program may use at most 64 MiB of HBM per device.

v0:
```python
import jax
import jax.numpy as jnp
from jax import lax
from jax.sharding import PartitionSpec as P

beta_mom = 0.9
learn_rate = 0.01


def contract(latent, cotangent):
    return lax.dot_general(
        latent, cotangent, (((0,), (0,)), ((), ())), preferred_element_type=jnp.float32
    )


def left_product(half, left_rows, site_query):

    def accumulate(piece):
        return jnp.dot(left_rows, piece, preferred_element_type=jnp.float32)

    if site_query:
        return accumulate(lax.all_gather(half, "fs", axis=0, tiled=True))
    return accumulate(lax.all_gather(half, "fs", axis=0, tiled=True))


def right_product(left_half, right, width):
    rows = left_half.shape[0]
    heads_here = right.shape[0]
    blocks = left_half.reshape(rows, heads_here, width)
    pre = jnp.einsum("rhd,hde->rhe", blocks, right, preferred_element_type=jnp.float32)
    return pre.reshape(rows, heads_here * width)


def on_device(
    saved_query_latent,
    saved_key_value_latent,
    query_cot,
    kv_cot,
    query_full_weight,
    key_value_full_weight,
    query_mom,
    kv_mom,
    query_left,
    kv_left,
    query_right,
    kv_right,
):
    query_terms = contract(lax.all_gather(saved_query_latent, "tp", axis=1, tiled=True), query_cot)
    latent_terms = contract(
        lax.all_gather(saved_key_value_latent, "tp", axis=1, tiled=True), kv_cot
    )
    query_grad = lax.psum_scatter(query_terms, "fs", scatter_dimension=0, tiled=True)
    kv_grad = lax.psum_scatter(latent_terms, "fs", scatter_dimension=0, tiled=True)
    query_mom_new = beta_mom * query_mom + query_grad
    kv_mom_new = beta_mom * kv_mom + kv_grad
    query_msq = jnp.sum(query_mom_new * query_mom_new)
    kv_msq = jnp.sum(kv_mom_new * kv_mom_new)
    query_msq, kv_msq = lax.psum((query_msq, kv_msq), ("fs", "tp"))
    query_pre_left = left_product(query_mom_new.astype(jnp.bfloat16), query_left, True)
    kv_pre_left = left_product(kv_mom_new.astype(jnp.bfloat16), kv_left, False)
    query_pre = right_product(
        query_pre_left.astype(jnp.bfloat16), query_right, query_right.shape[1]
    )
    kv_pre = right_product(kv_pre_left.astype(jnp.bfloat16), kv_right, kv_right.shape[1])
    query_psq = jnp.sum(query_pre * query_pre)
    kv_psq = jnp.sum(kv_pre * kv_pre)
    query_psq, kv_psq = lax.psum((query_psq, kv_psq), ("fs", "tp"))
    query_update = jnp.sqrt(query_msq / query_psq) * query_pre
    kv_update = jnp.sqrt(kv_msq / kv_psq) * kv_pre
    query_weight = query_full_weight - learn_rate * query_update
    kv_weight = key_value_full_weight - learn_rate * kv_update
    query_copy, kv_copy = (
        lax.all_gather(query_weight.astype(jnp.bfloat16), "fs", axis=0, tiled=True),
        lax.all_gather(kv_weight.astype(jnp.bfloat16), "fs", axis=0, tiled=True),
    )
    return (
        query_mom_new,
        kv_mom_new,
        query_update,
        kv_update,
        query_weight,
        kv_weight,
        query_copy,
        kv_copy,
    )


def solution(mesh):
    placed = (
        P("fs", "tp"),
        P("fs", "tp"),
        P("fs", "tp"),
        P("fs", "tp"),
        P("fs", "tp"),
        P("fs", "tp"),
        P("fs", "tp"),
        P("fs", "tp"),
        P("fs", None),
        P("fs", None),
        P("tp", None, None),
        P("tp", None, None),
    )
    return jax.shard_map(
        on_device,
        mesh=mesh,
        in_specs=placed,
        out_specs=(
            P("fs", "tp"),
            P("fs", "tp"),
            P("fs", "tp"),
            P("fs", "tp"),
            P("fs", "tp"),
            P("fs", "tp"),
            P(None, "tp"),
            P(None, "tp"),
        ),
        check_vma=False,
    )
```

profile of v0, /device:TPU:0, one launch (start us, length us, event | category | flops | bytes accessed | tf_op | source)
XLA Modules:
  0.0 414.4 jit_solution(13720712923901318106)
XLA Ops:
  7.2 0.0 copy-start
  7.2 0.0 all-gather.9.cloned.1.call-start
  7.2 0.7 all-gather.9.cloned.1.call-update
  7.9 0.0 all-gather.7.cloned.1.call-start
  8.0 0.7 all-gather.7.cloned.1.call-update
  8.7 0.0 reduce-scatter.5.cloned.1.call-start
  8.7 34.2 %all-gather.9.cloned.1.call-done = bf16[1024,1024]{1,0:T(8,128)(2,1)} async-done(((bf16[1024,128]{1,0:T(8,128)(2,1)}), bf16[1024,1024]{1,0:T(8,128)(2,1)}) %all-gather.9.cloned.1.call-update) | async-done | bytes 2097168 | tf_op jit(solution)/shard_map/all_gather | solution.py:50
  42.9 0.0 copy-done
  43.0 6.0 %fusion.4 = f32[1024,1024]{1,0:T(8,128)} fusion(bf16[1024,1024]{1,0:T(8,128)(2,1)} %all-gather.9.cloned.1.call-done, bf16[1024,1024]{1,0:T(8,128)(2,1)S(1)} %copy-done), kind=kOutput, calls=%fused_computation.16 | convolution fusion | flops 2147483648 | bytes 8388608 | tf_op jit(solution)/shard_map/dot_general | solution.py:11
  48.9 0.0 reduce-scatter.5.cloned.1.call-update
  49.0 0.0 reduce-scatter.3.cloned.1.call-start
  49.0 32.8 %all-gather.7.cloned.1.call-done = bf16[1024,1536]{0,1:T(8,128)(2,1)} async-done(((bf16[1024,192]{0,1:T(8,128)(2,1)}), bf16[1024,1536]{0,1:T(8,128)(2,1)}) %all-gather.7.cloned.1.call-update) | async-done | bytes 3145744 | tf_op jit(solution)/shard_map/all_gather | solution.py:48
  81.8 7.1 %fusion.3 = f32[1536,768]{1,0:T(8,128)} fusion(bf16[1024,1536]{0,1:T(8,128)(2,1)} %all-gather.7.cloned.1.call-done, bf16[1024,768]{1,0:T(8,128)(2,1)} %param.14), kind=kOutput, calls=%fused_computation.15 | convolution fusion | flops 2415919104 | bytes 9437184 | tf_op jit(solution)/shard_map/dot_general | solution.py:11
  88.9 0.0 reduce-scatter.3.cloned.1.call-update
  89.0 0.0 all-gather.13.cloned.1.call-start
  89.0 47.3 %reduce-scatter.5.cloned.1.call-done = f32[256,1024]{1,0:T(8,128)} async-done(((f32[1024,1024]{1,0:T(8,128)}), f32[256,1024]{1,0:T(8,128)}) %reduce-scatter.5.cloned.1.call-update) | async-done | bytes 1048592 | tf_op jit(solution)/shard_map/reduce_scatter | solution.py:53
  136.4 2.5 fusion.2
  138.9 0.0 all-gather.13.cloned.1.call-update
  138.9 0.0 all-gather.11.cloned.1.call-start
  139.0 57.2 %reduce-scatter.3.cloned.1.call-done = f32[384,768]{1,0:T(8,128)} async-done(((f32[1536,768]{1,0:T(8,128)}), f32[384,768]{1,0:T(8,128)}) %reduce-scatter.3.cloned.1.call-update) | async-done | bytes 1179664 | tf_op jit(solution)/shard_map/reduce_scatter | solution.py:52
  196.2 2.5 multiply_reduce_fusion.1
  198.8 1.0 copy-done.1
  199.8 0.9 convert_element_type.24
  200.7 0.0 all-gather.11.cloned.1.call-update
  200.7 0.0 all-gather.17.cloned.1.call-start
  200.7 0.9 multiply_reduce_fusion.3
  201.6 32.1 %all-gather.13.cloned.1.call-done = bf16[1024,1024]{1,0:T(8,128)(2,1)} async-done(((bf16[256,1024]{1,0:T(8,128)(2,1)}), bf16[1024,1024]{1,0:T(8,128)(2,1)}) %all-gather.13.cloned.1.call-update) | async-done | bytes 2097168 | tf_op jit(solution)/shard_map/all_gather | solution.py:23
  233.7 2.4 convolution_convert_fusion.1
  236.1 2.0 multiply_reduce_fusion.2
  238.1 35.2 %all-gather.11.cloned.1.call-done = bf16[1536,768]{1,0:T(8,128)(2,1)} async-done(((bf16[384,768]{1,0:T(8,128)(2,1)}), bf16[1536,768]{1,0:T(8,128)(2,1)}) %all-gather.11.cloned.1.call-update) | async-done | bytes 2359312 | tf_op jit(solution)/shard_map/all_gather | solution.py:22
  273.3 3.5 convolution_convert_fusion
  276.8 1.2 multiply_reduce_fusion
  278.0 39.7 %all-reduce = (f32[]{:T(128)}, f32[]{:T(128)}, f32[]{:T(128)}, f32[]{:T(128)}) all-reduce(f32[]{:T(128)} %get-tuple-element.26, f32[]{:T(128)} %get-tuple-element.28, f32[]{:T(128)} %multiply_reduce_fusion.3, f32[]{:T(128)} %get-tuple-element.30), channel_id=1, replica_groups=mesh['fs'=4,'tp'=8] {'fs','tp'}, use_global_device_ids=true, to_apply=%region_3.0 | all-reduce | flops 4 | bytes 32 | tf_op jit(solution)/shard_map/psum | solution.py:58
  319.0 2.3 broadcast_multiply_fusion.1
  321.3 2.5 copy.26
  323.8 3.0 fusion
  326.8 0.0 all-gather.17.cloned.1.call-update
  326.8 0.0 all-gather.15.cloned.1.call-start
  328.2 1.1 broadcast_multiply_fusion
  329.2 1.6 copy.25
  330.9 0.0 copy-start.2
  330.9 3.1 fusion.1
  334.0 0.0 copy-done.2
  334.0 0.0 all-gather.15.cloned.1.call-update
  334.0 29.1 %all-gather.17.cloned.1.call-done = bf16[1024,1024]{1,0:T(8,128)(2,1)} async-done(((bf16[256,1024]{1,0:T(8,128)(2,1)}), bf16[1024,1024]{1,0:T(8,128)(2,1)}) %all-gather.17.cloned.1.call-update) | async-done | bytes 2097168 | tf_op jit(solution)/shard_map/all_gather | solution.py:74
  363.1 39.8 %all-gather.15.cloned.1.call-done = bf16[1536,768]{1,0:T(8,128)(2,1)} async-done(((bf16[384,768]{1,0:T(8,128)(2,1)}), bf16[1536,768]{1,0:T(8,128)(2,1)}) %all-gather.15.cloned.1.call-update) | async-done | bytes 2359312 | tf_op jit(solution)/shard_map/all_gather | solution.py:73
  402.9 3.4 copy.32
  406.3 1.3 copy.33
  (9 shorter events, 0.0 us)
Async XLA Ops:
  7.2 35.8 %copy-start = (bf16[1024,1024]{1,0:T(8,128)(2,1)S(1)}, bf16[1024,1024]{1,0:T(8,128)(2,1)}, u32[]{:S(2)}) copy-start(bf16[1024,1024]{1,0:T(8,128)(2,1)} %param.15) | copy-start | bytes 6291460
  7.2 35.8 %all-gather.9.cloned.1.call-start = ((), (), s32[]{:S(2)}) async-start(), calls=%async_computation.4 | async-start | bytes 2359296 | tf_op jit(solution)/shard_map/all_gather | solution.py:50
  7.9 73.9 %all-gather.7.cloned.1.call-start = ((), (), s32[]{:S(2)}) async-start(), calls=%async_computation.2 | async-start | bytes 3538944 | tf_op jit(solution)/shard_map/all_gather | solution.py:48
  8.7 127.7 %reduce-scatter.5.cloned.1.call-start = ((), (), s32[]{:S(2)}) async-start(), calls=%async_computation.5 | async-start | bytes 5242880 | tf_op jit(solution)/shard_map/reduce_scatter | solution.py:53
  49.0 147.3 %reduce-scatter.3.cloned.1.call-start = ((), (), s32[]{:S(2)}) async-start(), calls=%async_computation.3 | async-start | bytes 5898240 | tf_op jit(solution)/shard_map/reduce_scatter | solution.py:52
  89.0 144.7 %all-gather.13.cloned.1.call-start = ((), (), s32[]{:S(2)}) async-start(), calls=%async_computation.7 | async-start | bytes 2621440 | tf_op jit(solution)/shard_map/all_gather | solution.py:23
  138.9 61.8 %copy-start.3 = (f32[256,1024]{1,0:T(8,128)}, f32[256,1024]{1,0:T(8,128)S(1)}, u32[]{:S(2)}) copy-start(f32[256,1024]{1,0:T(8,128)S(1)} %get-tuple-element.41) | copy-start | bytes 3145732
  138.9 134.4 %all-gather.11.cloned.1.call-start = ((), (), s32[]{:S(2)}) async-start(), calls=%async_computation.6 | async-start | bytes 2949120 | tf_op jit(solution)/shard_map/all_gather | solution.py:22
  198.8 1.0 copy-start.1
  200.7 162.4 %all-gather.17.cloned.1.call-start = ((), (), s32[]{:S(2)}) async-start(), calls=%async_computation.9 | async-start | bytes 2621440 | tf_op jit(solution)/shard_map/all_gather | solution.py:74
  201.6 34.5 %copy-start.5 = (bf16[4,256,256]{2,1,0:T(8,128)(2,1)S(1)}, bf16[4,256,256]{2,1,0:T(8,128)(2,1)}, u32[]{:S(2)}) copy-start(bf16[4,256,256]{2,1,0:T(8,128)(2,1)} %param.23) | copy-start | bytes 1572868
  273.3 3.5 copy-start.6
  326.8 76.0 %all-gather.15.cloned.1.call-start = ((), (), s32[]{:S(2)}) async-start(), calls=%async_computation.8 | async-start | bytes 2949120 | tf_op jit(solution)/shard_map/all_gather | solution.py:73
  330.9 3.1 copy-start.2
  402.9 3.4 copy-start.4
Sparse Core Ops, SparseCore 0:
  9.6 33.3 all-gather.8
  44.6 37.2 all-gather.6
  84.8 51.5 reduce-scatter.4
  139.2 56.9 reduce-scatter.2
  198.5 35.1 all-gather.12
  236.0 37.3 all-gather.10
  326.9 36.0 all-gather.16
  365.5 37.3 all-gather.14
where the time goes:
time: 415 us; the launch traced here: 414 us
  waiting for transfers between devices  309 us (74%)
  blocking collectives  39.7 us (10%)
  matrix products  22.1 us (5%)
  between operations  16.9 us (4%)
  other arithmetic  16.2 us (4%)
  local copies, waits for them, and re-layouts  9.9 us (2%)
    all_gather x2, waiting for transfers between devices, left_product(): return accumulate(lax.all_gather(half, 'fs', axis=0, tiled=True))  67.3 us
    reduce_scatter x1, waiting for transfers between devices, on_device(): lax.psum_scatter(query_terms, 'fs', scatter_dimension=0, tiled=True)  57.2 us
    reduce_scatter x1, waiting for transfers between devices, on_device(): lax.psum_scatter(latent_terms, 'fs', scatter_dimension=0, tiled=True)  47.3 us
    all_gather x1, waiting for transfers between devices, on_device(): lax.all_gather(query_weight.astype(jnp.bfloat16), 'fs', axis=0, tiled=True)  39.8 us
    psum x1, blocking collectives, on_device(): query_msq, kv_msq = lax.psum((query_msq, kv_msq), ('fs', 'tp'))  39.7 us
    all_gather x1, waiting for transfers between devices, on_device(): lax.all_gather(saved_key_value_latent, 'tp', axis=1, tiled=True)  34.2 us
    all_gather x1, waiting for transfers between devices, on_device(): lax.all_gather(saved_query_latent, 'tp', axis=1, tiled=True)  32.8 us
    all_gather x1, waiting for transfers between devices, on_device(): lax.all_gather(kv_weight.astype(jnp.bfloat16), 'fs', axis=0, tiled=True)  29.1 us
  transfers between devices with their start and end apart: 8, of which 8 were waited for; matrix products, arithmetic and copies ran while one was open for 7% of the time, Pallas kernels for 0%

commit v1 on v0

v1 whole, which is shorter than its diff:
```python
import functools

import jax
import jax.numpy as jnp
from jax import lax
from jax.experimental import pallas as pl
from jax.experimental.pallas import tpu as pltpu
from jax.sharding import PartitionSpec as P

MESH = pl.DeviceIdType.MESH
beta_mom = 0.9
learn_rate = 0.01


def col_tile(cols):
    return 256 if cols % 256 == 0 else cols


def rcopy(src, dst, send, recv, dev):
    return pltpu.make_async_remote_copy(
        src_ref=src, dst_ref=dst, send_sem=send, recv_sem=recv, device_id=dev, device_id_type=MESH
    )


def kernel(nf, nt, *refs):
    (lat, cot_h, w_h, mom_h, left_h, right_h) = [refs[2 * i : 2 * i + 2] for i in range(6)]
    outs = refs[12:20]
    mom_o, upd_o, wgt_o, cpy_o = [outs[2 * i : 2 * i + 2] for i in range(4)]
    s = refs[20:]
    cot, w, mom, left, right, lat_all, own, pb, rb, half, pre, cpy, stf, stt, st0, st1 = [
        s[2 * i : 2 * i + 2] for i in range(16)
    ]
    (in_sem, out_sem, bar_a_up, a_dn, a_sib_u, a_sib_d, a_recv, b_send, b_recv, g_send, g_recv,
     sf_send, sf_recv, st_send, st_recv) = s[32:]
    a_up = bar_a_up

    f = lax.axis_index("fs")
    t = lax.axis_index("tp")
    nz = nt // 2
    z = t // 2
    c = t % 2
    sib = z * 2 + (1 - c)

    loads = []
    for m in range(2):
        for i, (src, dst) in enumerate(
            [(cot_h[m], cot[m]), (mom_h[m], mom[m]), (left_h[m], left[m]), (right_h[m], right[m]), (w_h[m], w[m])]
        ):
            cp = pltpu.make_async_copy(src, dst, in_sem.at[m, i])
            cp.start()
            loads.append(cp)
    load = lambda m, i: loads[5 * m + i]

    rt = [lat[m].shape[0] for m in range(2)]
    rows = [2 * r for r in rt]
    cols = [cot[m].shape[1] for m in range(2)]

    def shard(m, k, core):
        return lat_all[m].at[k, pl.ds(pl.multiple_of(core * rt[m], rt[m]), rt[m])]

    local = []
    for m in range(2):
        cp = pltpu.make_async_copy(lat[m], shard(m, z, c), in_sem.at[m, 5])
        cp.start()
        local.append(cp)

    barrier = pltpu.get_barrier_semaphore()
    for d in range(1, nf):
        pl.semaphore_signal(barrier, inc=1, device_id={"fs": (f + d) % nf}, device_id_type=MESH)
    for d in range(1, nt):
        pl.semaphore_signal(barrier, inc=1, device_id={"tp": (t + d) % nt}, device_id_type=MESH)
    pl.semaphore_wait(barrier, nf + nt - 2)

    def up(m, i, k, src=None):
        return rcopy(
            shard(m, k, c) if src is None else src, shard(m, k, c), a_up.at[m, i], a_recv.at[m, k, c], {"tp": t + 2}
        )

    def down(m, i, k, src=None):
        return rcopy(
            shard(m, k, c) if src is None else src, shard(m, k, c), a_dn.at[m, i], a_recv.at[m, k, c], {"tp": t - 2}
        )

    def across(m, sem, k, src=None):
        return rcopy(
            shard(m, k, c) if src is None else src, shard(m, k, c), sem, a_recv.at[m, k, c], {"tp": sib}
        )

    def own_up(m):
        @pl.when(z < nz - 1)
        def _():
            up(m, 0, z, lat[m]).start()

    def own_down(m):
        @pl.when(z > 0)
        def _():
            down(m, 0, z, lat[m]).start()

    def wait_shard(m, k, core):
        x = shard(m, k, core)
        rcopy(x, x, a_up.at[m, 0], a_recv.at[m, k, core], {"tp": sib}).wait_recv()

    def partial(m, k):
        tile = col_tile(cols[m])

        def body(i, carry):
            cs = pl.ds(pl.multiple_of(i * tile, tile), tile)
            p = jnp.dot(lat_all[m][k], cot[m][:, cs], preferred_element_type=jnp.float32)

            @pl.when(k == f)
            def _():
                own[m][:, cs] = p

            @pl.when(k != f)
            def _():
                pb[m][k, :, cs] = p.astype(jnp.bfloat16)

            return carry

        lax.fori_loop(0, cols[m] // tile, body, 0)

        @pl.when(k != f)
        def _():
            rcopy(pb[m].at[k], rb[m].at[f], b_send.at[m, k], b_recv.at[m, f], {"fs": k}).start()

    own_up(0)
    own_down(0)
    for m in range(2):
        across(m, a_sib_u.at[m, 0], z, lat[m]).start()

    for m in range(2):
        if m == 0:
            pl.when(z == 0)(lambda: own_up(1))
            pl.when(z == nz - 1)(lambda: own_down(1))
        load(m, 0).wait()
        local[m].wait()
        wait_shard(m, z, 1 - c)
        partial(m, z)

        def step(i, carry, m=m):
            lo, hi = z - i, z + i

            @pl.when(lo >= 0)
            def _():
                wait_shard(m, lo, c)

                @pl.when(z < nz - 1)
                def _():
                    up(m, i, lo).start()

                across(m, a_sib_u.at[m, i], lo).start()

            @pl.when(hi < nz)
            def _():
                wait_shard(m, hi, c)

                @pl.when(z > 0)
                def _():
                    down(m, i, hi).start()

                across(m, a_sib_d.at[m, i], hi).start()

            if m == 0:
                pl.when(z == i)(lambda: own_up(1))
                pl.when(z == nz - 1 - i)(lambda: own_down(1))

            @pl.when(lo >= 0)
            def _():
                wait_shard(m, lo, 1 - c)
                partial(m, lo)

            @pl.when(hi < nz)
            def _():
                wait_shard(m, hi, 1 - c)
                partial(m, hi)

            return carry

        lax.fori_loop(1, nz, step, 0)

    relay = nf == 4
    xn = (f // 2) * 2 + (1 - f % 2)
    yn = (1 - f // 2) * 2 + f % 2
    dn = 3 - f

    def block(buf, m, g, part=None):
        r = rows[m]
        if part is None:
            return buf[m].at[pl.ds(pl.multiple_of(g * r, r), r)]
        return buf[m].at[pl.ds(pl.multiple_of(g * r + part * (r // 2), r // 2), r // 2)]

    def g_copy(ph, buf, m, i, g, dev, part=None):
        b = block(buf, m, g, part)
        return rcopy(b, b, g_send.at[ph, m, i], g_recv.at[ph, m, i], {"fs": dev})

    def gather_own(ph, buf, m):
        if relay:
            g_copy(ph, buf, m, 0, f, xn).start()
            g_copy(ph, buf, m, 1, f, yn).start()
        else:
            for d in range(1, nf):
                g_copy(ph, buf, m, d, f, (f + d) % nf).start()

    def gather_forward(ph, buf, m):
        if relay:
            g_copy(ph, buf, m, 0, xn, xn).wait_recv()
            g_copy(ph, buf, m, 2, xn, yn, 0).start()
            g_copy(ph, buf, m, 1, yn, yn).wait_recv()
            g_copy(ph, buf, m, 3, yn, xn, 1).start()

    def gather_finish(ph, buf, m):
        if relay:
            g_copy(ph, buf, m, 2, dn, yn, 0).wait_recv()
            g_copy(ph, buf, m, 3, dn, xn, 1).wait_recv()
        else:
            for d in range(1, nf):
                g_copy(ph, buf, m, d, (f + nf - d) % nf, f).wait_recv()

    def gather_drain(ph, buf, m):
        if relay:
            g_copy(ph, buf, m, 0, f, xn).wait_send()
            g_copy(ph, buf, m, 1, f, yn).wait_send()
            g_copy(ph, buf, m, 2, xn, yn, 0).wait_send()
            g_copy(ph, buf, m, 3, yn, xn, 1).wait_send()
        else:
            for d in range(1, nf):
                g_copy(ph, buf, m, d, f, (f + d) % nf).wait_send()

    def reduce_momentum(m):
        load(m, 1).wait()
        for d in range(1, nf):
            g = (f + d) % nf
            rcopy(rb[m].at[g], rb[m].at[g], b_send.at[m, 0], b_recv.at[m, g], {"fs": g}).wait_recv()
        tile = col_tile(cols[m])
        r = rows[m]

        def body(i, acc):
            cs = pl.ds(pl.multiple_of(i * tile, tile), tile)
            g = own[m][:, cs]
            for d in range(1, nf):
                g = g + rb[m][(f + d) % nf, :, cs].astype(jnp.float32)
            new = beta_mom * mom[m][:, cs] + g
            mom[m][:, cs] = new
            half[m][pl.ds(pl.multiple_of(f * r, r), r), cs] = new.astype(jnp.bfloat16)
            return acc + jnp.sum(new * new, axis=0, keepdims=True)

        acc = lax.fori_loop(0, cols[m] // tile, body, jnp.zeros((1, tile), jnp.float32))
        gather_own(0, half, m)
        pltpu.make_async_copy(mom[m], mom_o[m], out_sem.at[m, 0]).start()
        return jnp.sum(acc)

    def direction(m, msq):
        load(m, 2).wait()
        load(m, 3).wait()
        width = right[m].shape[1]

        def body(i, acc):
            cs = pl.ds(pl.multiple_of(i * width, width), width)
            lh = jnp.dot(left[m][...], half[m][:, cs], preferred_element_type=jnp.float32)
            p = jnp.dot(lh.astype(jnp.bfloat16), right[m][i], preferred_element_type=jnp.float32)
            pre[m][:, cs] = p
            return acc + jnp.sum(p * p, axis=0, keepdims=True)

        acc = lax.fori_loop(0, cols[m] // width, body, jnp.zeros((1, width), jnp.float32))
        st0[m][0:8, :] = jnp.full((8, 128), msq, jnp.float32)
        st0[m][8:16, :] = jnp.full((8, 128), jnp.sum(acc), jnp.float32)
        for d in range(1, nt):
            rcopy(st0[m], stt[m].at[d], st_send.at[m, d], st_recv.at[m, d], {"tp": (t + d) % nt}).start()

    def stats_tp(m):
        tot = st0[m][...]
        for d in range(1, nt):
            rcopy(st0[m], stt[m].at[d], st_send.at[m, d], st_recv.at[m, d], {"tp": sib}).wait_recv()
            tot = tot + stt[m][d]
        st1[m][...] = tot
        for d in range(1, nf):
            rcopy(st1[m], stf[m].at[d], sf_send.at[m, d], sf_recv.at[m, d], {"fs": (f + d) % nf}).start()

    def finish(m):
        tot = st1[m][...]
        for d in range(1, nf):
            rcopy(st1[m], stf[m].at[d], sf_send.at[m, d], sf_recv.at[m, d], {"fs": f}).wait_recv()
            tot = tot + stf[m][d]
        scale = jnp.sqrt(tot[0:1, 0:1] / tot[8:9, 0:1])
        load(m, 4).wait()
        tile = col_tile(cols[m])
        r = rows[m]

        def body(i, carry):
            cs = pl.ds(pl.multiple_of(i * tile, tile), tile)
            u = scale * pre[m][:, cs]
            new = w[m][:, cs] - learn_rate * u
            pre[m][:, cs] = u
            w[m][:, cs] = new
            cpy[m][pl.ds(pl.multiple_of(f * r, r), r), cs] = new.astype(jnp.bfloat16)
            return carry

        lax.fori_loop(0, cols[m] // tile, body, 0)
        gather_own(1, cpy, m)
        pltpu.make_async_copy(pre[m], upd_o[m], out_sem.at[m, 1]).start()
        pltpu.make_async_copy(w[m], wgt_o[m], out_sem.at[m, 2]).start()

    msq0 = reduce_momentum(0)
    msq1 = reduce_momentum(1)
    gather_forward(0, half, 0)
    gather_finish(0, half, 0)
    direction(0, msq0)
    gather_forward(0, half, 1)
    stats_tp(0)
    finish(0)
    gather_finish(0, half, 1)
    direction(1, msq1)
    stats_tp(1)
    gather_forward(1, cpy, 0)
    finish(1)
    gather_finish(1, cpy, 0)
    pltpu.make_async_copy(cpy[0], cpy_o[0], out_sem.at[0, 3]).start()
    gather_forward(1, cpy, 1)
    gather_finish(1, cpy, 1)
    pltpu.make_async_copy(cpy[1], cpy_o[1], out_sem.at[1, 3]).start()

    for m in range(2):
        gather_drain(0, half, m)
        gather_drain(1, cpy, m)
        for d in range(1, nt):
            rcopy(st0[m], stt[m].at[d], st_send.at[m, d], st_recv.at[m, d], {"tp": (t + d) % nt}).wait_send()
        for d in range(1, nf):
            rcopy(st1[m], stf[m].at[d], sf_send.at[m, d], sf_recv.at[m, d], {"fs": (f + d) % nf}).wait_send()
            g = (f + d) % nf
            rcopy(pb[m].at[g], rb[m].at[f], b_send.at[m, g], b_recv.at[m, f], {"fs": g}).wait_send()

        across(m, a_sib_u.at[m, 0], z).wait_send()

        def drain(i, carry, m=m):
            lo, hi = z - i, z + i

            @pl.when((lo >= 0) & (z < nz - 1))
            def _():
                up(m, i, lo).wait_send()

            @pl.when((hi < nz) & (z > 0))
            def _():
                down(m, i, hi).wait_send()

            @pl.when((lo >= 0) & (i > 0))
            def _():
                across(m, a_sib_u.at[m, i], lo).wait_send()

            @pl.when((hi < nz) & (i > 0))
            def _():
                across(m, a_sib_d.at[m, i], hi).wait_send()

            return carry

        lax.fori_loop(0, nz, drain, 0)
        for i, (src, dst) in enumerate([(mom[m], mom_o[m]), (pre[m], upd_o[m]), (w[m], wgt_o[m]), (cpy[m], cpy_o[m])]):
            pltpu.make_async_copy(src, dst, out_sem.at[m, i]).wait()


def paired(right):
    heads, width = right.shape[0], right.shape[1]
    if width % 128 == 0 or heads % 2:
        return right
    a, b = right[0::2], right[1::2]
    zero = jnp.zeros_like(a)
    return jnp.concatenate(
        [jnp.concatenate([a, zero], axis=2), jnp.concatenate([zero, b], axis=2)], axis=1
    )


def on_device(nf, nt, q_lat, kv_lat, q_cot, kv_cot, q_w, kv_w, q_mom, kv_mom, q_left, kv_left, q_right, kv_right):
    lats = (kv_lat.T, q_lat.T)
    cots, ws, moms, lefts = (kv_cot, q_cot), (kv_w, q_w), (kv_mom, q_mom), (kv_left, q_left)
    rights = (paired(kv_right), paired(q_right))
    bf, f32 = jnp.bfloat16, jnp.float32
    sds = jax.ShapeDtypeStruct
    f32_out = [sds(x.shape, f32) for x in ws]
    cpy_out = [sds((x.shape[0] * nf, x.shape[1]), bf) for x in ws]
    V = pltpu.VMEM
    nz = nt // 2

    def both(make):
        return [make(m) for m in range(2)]

    scratch = (
        both(lambda m: V(cots[m].shape, bf))
        + both(lambda m: V(ws[m].shape, f32))
        + both(lambda m: V(moms[m].shape, f32))
        + both(lambda m: V(lefts[m].shape, bf))
        + both(lambda m: V(rights[m].shape, bf))
        + both(lambda m: V((nz, 2 * lats[m].shape[0], lats[m].shape[1]), bf))
        + both(lambda m: V(ws[m].shape, f32))
        + both(lambda m: V((nf,) + ws[m].shape, bf))
        + both(lambda m: V((nf,) + ws[m].shape, bf))
        + both(lambda m: V(cpy_out[m].shape, bf))
        + both(lambda m: V(ws[m].shape, f32))
        + both(lambda m: V(cpy_out[m].shape, bf))
        + both(lambda m: V((nf, 16, 128), f32))
        + both(lambda m: V((nt, 16, 128), f32))
        + both(lambda m: V((16, 128), f32))
        + both(lambda m: V((16, 128), f32))
    )
    D = pltpu.SemaphoreType.DMA
    ng = max(nf, 4)
    sems = [
        D((2, 6)), D((2, 4)), D((2, nz)), D((2, nz)), D((2, nz)), D((2, nz)), D((2, nz, 2)),
        D((2, nf)), D((2, nf)), D((2, 2, ng)), D((2, 2, ng)),
        D((2, nf)), D((2, nf)), D((2, nt)), D((2, nt)),
    ]
    any_spec = pl.BlockSpec(memory_space=pl.ANY)
    vmem_spec = pl.BlockSpec(memory_space=pltpu.VMEM)
    out = pl.pallas_call(
        functools.partial(kernel, nf, nt),
        out_shape=f32_out + f32_out + f32_out + cpy_out,
        in_specs=[vmem_spec] * 2 + [any_spec] * 10,
        out_specs=[any_spec] * 8,
        scratch_shapes=scratch + sems,
        compiler_params=pltpu.CompilerParams(
            collective_id=0, has_side_effects=True, vmem_limit_bytes=60 * 1024 * 1024
        ),
    )(*lats, *cots, *ws, *moms, *lefts, *rights)
    return (out[1], out[0], out[3], out[2], out[5], out[4], out[7], out[6])


def solution(mesh):
    nf, nt = mesh.shape["fs"], mesh.shape["tp"]
    placed = (P("fs", "tp"),) * 8 + (P("fs", None),) * 2 + (P("tp", None, None),) * 2
    return jax.shard_map(
        functools.partial(on_device, nf, nt),
        mesh=mesh,
        in_specs=placed,
        out_specs=(P("fs", "tp"),) * 6 + (P(None, "tp"),) * 2,
        check_vma=False,
    )
```

time: 415 us -> 186 us (0.45)
  waiting for transfers between devices: 309 us -> 0 us
  Pallas kernels: 0 us -> 167 us
  blocking collectives: 39.7 us -> 0 us
  matrix products: 22.1 us -> 0 us
  between operations: 16.9 us -> 0.66 us
  other arithmetic: 16.2 us -> 0.94 us
  local copies, waits for them, and re-layouts: 9.9 us -> 16.4 us
    all_gather x6 -> x0, waiting for transfers between devices: 203 us -> none  [the longest x2 67.3 us: left_product(): return accumulate(lax.all_gather(half, 'fs', axis=0, tiled=True))]
    pallas_call x0 -> x1, Pallas kernels: none -> 167 us  [on_device(): pl.pallas_call(functools.partial(kernel, nf, nt), out_shape=f32_out + f32...]
    reduce_scatter x2 -> x0, waiting for transfers between devices: 105 us -> none  [the longest x1 57.2 us: on_device(): lax.psum_scatter(query_terms, 'fs', scatter_dimension=0, tiled=True)]
    psum x1 -> x0, blocking collectives: 39.7 us -> none  [on_device(): query_msq, kv_msq = lax.psum((query_msq, kv_msq), ('fs', 'tp'))]
    dot_general x6 -> x0, matrix products: 22.1 us -> none  [the longest x2 13.1 us: contract(): lax.dot_general(latent, cotangent, (((0,), (0,)), ((), ())), preferred_el...]
    convert_element_type x4 -> x0, other arithmetic: 9.44 us -> none  [the longest x1 3.05 us: on_device(): query_weight.astype(jnp.bfloat16)]
    unnamed x18 -> x23, local copies, waits for them, and re-layouts: 9.9 us -> 15.4 us
  transfers between devices with their start and end apart: 8 -> 0, of which waited for: 8 -> 0; matrix products, arithmetic and copies ran while one was open for 7% -> 0% of each run, Pallas kernels for 0% -> 0%
where the time goes in v1:
time: 186 us; the launch traced here: 185 us
  Pallas kernels  167 us (90%)
  local copies, waits for them, and re-layouts  16.4 us (9%)
    pallas_call x1, Pallas kernels, on_device(): pl.pallas_call(functools.partial(kernel, nf, nt), out_shape=f32_out + f32...  167 us
    unnamed x23, local copies, waits for them, and re-layouts  15.4 us

profile of v1, /device:TPU:0, one launch (start us, length us, event | category | flops | bytes accessed | tf_op | source)
XLA Modules:
  0.0 185.1 jit_solution(3715419184157180006)
XLA Ops:
  0.6 1.8 copy.20
  2.4 1.0 fusion.3
  3.5 0.9 fusion.2.refs_11_
  4.4 167.1 %shard_map.179 = (f32[256,1024]{1,0:T(8,128)}, f32[384,768]{1,0:T(8,128)}, f32[256,1024]{1,0:T(8,128)}, f32[384,768]{1,0:T(8,128)}, f32[256,1024]{1,0:T(8,128)},...) custom-call(bf16[128,1024]{1,0:T(8,128)(2,1)} %bitcast.2, bf16[192,1024]{1,0:T(8,128)(2,1)} %bitcast.3, ...), custom_call_target="tpu_custom_call" | custom-call | tf_op jit(solution)/shard_map/pallas_call | solution.py:412
  171.5 0.0 copy-start.6
  171.5 2.4 %copy.29 = f32[384,768]{1,0:T(8,128)} copy(f32[384,768]{1,0:T(8,128)} %get-tuple-element.34) | data formatting | bytes 2359296
  174.0 0.0 copy-done.6
  174.0 0.0 copy-start.3
  174.0 1.0 copy.30
  175.0 0.7 copy-done.3
  175.6 0.0 copy-start.5
  175.6 1.0 copy.31
  176.7 0.6 copy-done.5
  177.3 0.0 copy-start.2
  177.3 0.0 copy-start.4
  177.3 1.0 copy.32
  178.3 0.7 copy-done.2
  178.9 0.0 copy-start
  178.9 1.0 copy.33
  180.0 0.0 copy-done.4
  180.0 1.0 copy.34
  180.9 0.4 copy-done
  181.4 0.0 copy-start.1
  181.4 1.4 copy.35
  182.8 1.0 copy-done.1
  183.8 1.3 copy.36
Async XLA Ops:
  171.5 2.5 %copy-start.6 = (f32[256,1024]{1,0:T(8,128)S(1)}, f32[256,1024]{1,0:T(8,128)}, u32[]{:S(2)}) copy-start(f32[256,1024]{1,0:T(8,128)} %get-tuple-element.35) | copy-start | bytes 3145732
  174.0 1.6 copy-start.3
  175.6 1.7 copy-start.5
  177.3 1.6 copy-start.2
  177.3 2.7 %copy-start.4 = (f32[256,1024]{1,0:T(8,128)S(1)}, f32[256,1024]{1,0:T(8,128)}, u32[]{:S(2)}) copy-start(f32[256,1024]{1,0:T(8,128)} %get-tuple-element.39) | copy-start | bytes 3145732
  178.9 2.4 %copy-start = (bf16[1536,768]{1,0:T(8,128)(2,1)S(1)}, bf16[1536,768]{1,0:T(8,128)(2,1)}, u32[]{:S(2)}) copy-start(bf16[1536,768]{1,0:T(8,128)(2,1)} %get-tuple-element.40) | copy-start | bytes 7077892
  181.4 2.4 %copy-start.1 = (bf16[1024,1024]{1,0:T(8,128)(2,1)S(1)}, bf16[1024,1024]{1,0:T(8,128)(2,1)}, u32[]{:S(2)}) copy-start(bf16[1024,1024]{1,0:T(8,128)(2,1)} %get-tuple-element.41) | copy-start | bytes 6291460

commit v2 on v1

--- a/solution.py
+++ b/solution.py
@@ -252,12 +252,21 @@
     def direction(m, msq):
         load(m, 2).wait()
         load(m, 3).wait()
-        width = right[m].shape[1]
+        head = right[m].shape[1]
+        pair = 2 if head % 128 and right[m].shape[0] % 2 == 0 else 1
+        width = pair * head
 
         def body(i, acc):
             cs = pl.ds(pl.multiple_of(i * width, width), width)
             lh = jnp.dot(left[m][...], half[m][:, cs], preferred_element_type=jnp.float32)
-            p = jnp.dot(lh.astype(jnp.bfloat16), right[m][i], preferred_element_type=jnp.float32)
+            lh = lh.astype(jnp.bfloat16)
+            p = jnp.concatenate(
+                [
+                    jnp.dot(lh[:, j * head : (j + 1) * head], right[m][pair * i + j], preferred_element_type=jnp.float32)
+                    for j in range(pair)
+                ],
+                axis=1,
+            )
             pre[m][:, cs] = p
             return acc + jnp.sum(p * p, axis=0, keepdims=True)
 
@@ -357,21 +366,10 @@
             pltpu.make_async_copy(src, dst, out_sem.at[m, i]).wait()
 
 
-def paired(right):
-    heads, width = right.shape[0], right.shape[1]
-    if width % 128 == 0 or heads % 2:
-        return right
-    a, b = right[0::2], right[1::2]
-    zero = jnp.zeros_like(a)
-    return jnp.concatenate(
-        [jnp.concatenate([a, zero], axis=2), jnp.concatenate([zero, b], axis=2)], axis=1
-    )
-
-
 def on_device(nf, nt, q_lat, kv_lat, q_cot, kv_cot, q_w, kv_w, q_mom, kv_mom, q_left, kv_left, q_right, kv_right):
     lats = (kv_lat.T, q_lat.T)
     cots, ws, moms, lefts = (kv_cot, q_cot), (kv_w, q_w), (kv_mom, q_mom), (kv_left, q_left)
-    rights = (paired(kv_right), paired(q_right))
+    rights = (kv_right, q_right)
     bf, f32 = jnp.bfloat16, jnp.float32
     sds = jax.ShapeDtypeStruct
     f32_out = [sds(x.shape, f32) for x in ws]

time: 186 us -> 184 us (0.989)
  no operation moved by 1% of the time
where the time goes in v2:
time: 184 us; the launch traced here: 183 us
  Pallas kernels  167 us (91%)
  local copies, waits for them, and re-layouts  15.4 us (8%)
    pallas_call x1, Pallas kernels, on_device(): pl.pallas_call(functools.partial(kernel, nf, nt), out_shape=f32_out + f32...  167 us
    unnamed x23, local copies, waits for them, and re-layouts  15.4 us

profile of v2, /device:TPU:0, one launch (start us, length us, event | category | flops | bytes accessed | tf_op | source)
XLA Modules:
  0.0 183.1 jit_solution(12637885125481700430)
XLA Ops:
  0.6 1.8 copy.20
  2.4 167.1 %shard_map.179 = (f32[256,1024]{1,0:T(8,128)}, f32[384,768]{1,0:T(8,128)}, f32[256,1024]{1,0:T(8,128)}, f32[384,768]{1,0:T(8,128)}, f32[256,1024]{1,0:T(8,128)},...) custom-call(bf16[128,1024]{1,0:T(8,128)(2,1)} %bitcast.2, bf16[192,1024]{1,0:T(8,128)(2,1)} %bitcast.3, ...), custom_call_target="tpu_custom_call" | custom-call | tf_op jit(solution)/shard_map/pallas_call | solution.py:410
  169.5 0.0 copy-start.6
  169.5 2.4 %copy.29 = f32[384,768]{1,0:T(8,128)} copy(f32[384,768]{1,0:T(8,128)} %get-tuple-element.32) | data formatting | bytes 2359296
  172.0 0.0 copy-done.6
  172.0 0.0 copy-start.3
  172.0 1.0 copy.30
  173.0 0.7 copy-done.3
  173.6 0.0 copy-start.5
  173.6 1.0 copy.31
  174.7 0.6 copy-done.5
  175.3 0.0 copy-start.2
  175.3 0.0 copy-start.4
  175.3 1.0 copy.32
  176.3 0.7 copy-done.2
  176.9 0.0 copy-start
  176.9 1.0 copy.33
  178.0 0.0 copy-done.4
  178.0 1.0 copy.34
  178.9 0.4 copy-done
  179.4 0.0 copy-start.1
  179.4 1.4 copy.35
  180.8 1.0 copy-done.1
  181.8 1.3 copy.36
Async XLA Ops:
  169.5 2.5 %copy-start.6 = (f32[256,1024]{1,0:T(8,128)S(1)}, f32[256,1024]{1,0:T(8,128)}, u32[]{:S(2)}) copy-start(f32[256,1024]{1,0:T(8,128)} %get-tuple-element.33) | copy-start | bytes 3145732
  172.0 1.6 copy-start.3
  173.6 1.7 copy-start.5
  175.3 1.6 copy-start.2
  175.3 2.7 %copy-start.4 = (f32[256,1024]{1,0:T(8,128)S(1)}, f32[256,1024]{1,0:T(8,128)}, u32[]{:S(2)}) copy-start(f32[256,1024]{1,0:T(8,128)} %get-tuple-element.37) | copy-start | bytes 3145732
  176.9 2.4 %copy-start = (bf16[1536,768]{1,0:T(8,128)(2,1)S(1)}, bf16[1536,768]{1,0:T(8,128)(2,1)}, u32[]{:S(2)}) copy-start(bf16[1536,768]{1,0:T(8,128)(2,1)} %get-tuple-element.38) | copy-start | bytes 7077892
  179.4 2.4 %copy-start.1 = (bf16[1024,1024]{1,0:T(8,128)(2,1)S(1)}, bf16[1024,1024]{1,0:T(8,128)(2,1)}, u32[]{:S(2)}) copy-start(bf16[1024,1024]{1,0:T(8,128)(2,1)} %get-tuple-element.39) | copy-start | bytes 6291460
